TPU v7x, 32 devices: a whole 2x2x4 slice. The times are simulated.
32 devices in a mesh: ep: 8 (over z, y), tp: 4 (over x, core).
Axes of the slice: x: 2, y: 2, z: 4, core: 2. Of those that a mesh axis runs over, the one named last changes fastest.
Arguments:
- queries: bfloat16 [4096, 1024], P('ep', 'tp'), may hold values from -6 to 6
- keys: bfloat16 [4096, 512], P('ep', 'tp'), may hold values from -6 to 6
- values: bfloat16 [4096, 512], P('ep', 'tp'), may hold values from -6 to 6
- forget_cache: float32 [8, 4096], P('tp'), may hold values from -412 to 0, as said below
- query_gain: float32 [128], replicated, may hold values from 0.6 to 6
- key_gain: float32 [128], replicated, may hold values from 0.6 to 6
- mixer_out: bfloat16 [1024, 2048], replicated, may hold values from -0.75 to 0.75
- expert_input: bfloat16 [4096, 2048], P(('ep', 'tp')), may hold values from -6 to 6
- norm_gain: float32 [2048], replicated, may hold values from 0.1 to 1.9
- routes: int32 [4096, 2], P(('ep', 'tp')), may hold values from 0 to 31, all different within a row; in each aligned block of 128 rows (0 to 127, 128 to 255, ...) at most 16 rows name the same one
- route_weights: float32 [4096, 2], P(('ep', 'tp')), may hold values from 0.1 to 1
- w_gate: bfloat16 [32, 2048, 1024], P('ep', None, 'tp'), may hold values from -0.125 to 0.125
- w_up: bfloat16 [32, 2048, 1024], P('ep', None, 'tp'), may hold values from -0.125 to 0.125
- w_down: bfloat16 [32, 2048, 1024], P('ep', None, 'tp'), may hold values from -0.1875 to 0.1875
Outputs:
- mixed: bfloat16 [4096, 2048], P(('ep', 'tp'))
- routed: bfloat16 [4096, 2048], P(('ep', 'tp'))
Inputs may be any that keep to these rules, and one draw needn't show every extreme that they name: `routes`: each row names 2 different experts; among the rows of one device no expert is named by more than 16 rows, a bound that some block reaches. `forget_cache`: never rises along the positions.
All inputs are finite; a program needn't handle non-finite values.
Results may differ from a plain program's by a relative error of at most 0.013.
The roundings to bfloat16 on the way count: a program that leaves them out, or rounds other values in their place, can miss the bound.
Values may be sent and summed in bfloat16 or wider, within the bound.
A program may use at most 128 MiB of HBM per device.

v0:
```python
import math
import jax
import jax.numpy as jnp
from jax import lax
from jax.sharding import PartitionSpec as P

EXPERTS = 32
CAP = 16
EPSILON = 1e-06
NEGATIVE = -1e30


def rms_scale(inputs, gain):
    inputs = inputs.astype(jnp.float32)
    return inputs * lax.rsqrt(jnp.mean(inputs * inputs, axis=-1, keepdims=True) + EPSILON) * gain


def attend(queries, keys, values, forget_cache, query_gain, key_gain):
    rows = queries.shape[0]
    head_dim = keys.shape[1]
    local_heads = forget_cache.shape[0]
    first = lax.axis_index("ep") * rows
    normed_q = rms_scale(queries.reshape(rows, local_heads, head_dim), query_gain).astype(
        jnp.bfloat16
    )
    normed_k = rms_scale(keys, key_gain).astype(jnp.bfloat16)
    scale = head_dim ** (-0.5)
    groups = [(normed_q, first + jnp.arange(rows, dtype=jnp.int32))]
    gate_sets = [jnp.take(forget_cache, position, axis=1) for _, position in groups]
    initial = tuple(
        (
            (
                jnp.full((local_heads, group_rows.shape[0]), NEGATIVE, jnp.float32),
                jnp.zeros((local_heads, group_rows.shape[0]), jnp.float32),
                jnp.zeros((local_heads, group_rows.shape[0], head_dim), jnp.float32),
            )
            for group_rows, _ in groups
        )
    )
    key_matrix_rows = lax.all_gather(normed_k, "ep", axis=0, tiled=True)
    value_rows = lax.all_gather(values, "ep", axis=0, tiled=True)
    length = key_matrix_rows.shape[0]
    width = math.gcd(length, 512)
    query_rows, query_pos = groups[0]
    query_gates = gate_sets[0]
    last_pos = jnp.max(query_pos)

    def one_block(number, inner):
        begin = number * width

        def update(current):
            highest, denom, accum = current
            block_keys = lax.dynamic_slice_in_dim(key_matrix_rows, number * width, width, 0)
            block_values = lax.dynamic_slice_in_dim(value_rows, number * width, width, 0)
            key_gates = lax.dynamic_slice_in_dim(forget_cache, begin, width, 1)
            scores = (
                jnp.einsum(
                    "qhd,kd->hqk", query_rows, block_keys, preferred_element_type=jnp.float32
                )
                * scale
            )
            scores = scores + query_gates[:, :, None] - key_gates[:, None, :]
            key_pos = begin + jnp.arange(width, dtype=jnp.int32)
            allowed = key_pos[None, :] <= query_pos[:, None]
            scores = jnp.where(allowed[None], scores, NEGATIVE)
            newest = jnp.maximum(highest, jnp.max(scores, axis=2))
            weights = jnp.where(allowed[None], jnp.exp(scores - newest[:, :, None]), 0.0)
            factor = jnp.exp(highest - newest)
            denom = denom * factor + jnp.sum(weights, axis=2)
            product = jnp.einsum(
                "hqk,kd->hqd",
                weights.astype(jnp.bfloat16),
                block_values,
                preferred_element_type=jnp.float32,
            )
            accum = accum * factor[:, :, None] + product
            return (newest, denom, accum)

        return lax.cond(begin <= last_pos, update, lambda current: current, inner)

    results = [lax.fori_loop(0, length // width, one_block, initial[0])]
    finals = tuple(results)
    outputs = [(accum / denom[:, :, None]).astype(jnp.bfloat16) for _, denom, accum in finals]
    return outputs[0]


def dispatch(expert_input, norm_gain, routes):
    rows = expert_input.shape[0]
    top = routes.shape[1]
    normed = rms_scale(expert_input, norm_gain).astype(jnp.bfloat16)
    flat = routes.reshape(-1)
    onehot = (flat[:, None] == jnp.arange(EXPERTS, dtype=jnp.int32)[None, :]).astype(jnp.int32)
    prior_state = jnp.cumsum(onehot, axis=0) - onehot
    rank = jnp.sum(prior_state * onehot, axis=1)
    slots = rank * EXPERTS + flat
    owner = (
        jnp.full((CAP * EXPERTS,), rows, jnp.int32)
        .at[slots]
        .set(jnp.arange(rows * top, dtype=jnp.int32) // top)
    )
    padded = jnp.concatenate([normed, jnp.zeros((1, normed.shape[1]), jnp.bfloat16)], axis=0)
    outgoing = padded[owner].reshape(CAP, EXPERTS, normed.shape[1])
    received = lax.all_to_all(outgoing, "ep", split_axis=1, concat_axis=0, tiled=True)
    return (received, slots)


def on_device(
    queries,
    keys,
    values,
    forget_cache,
    query_gain,
    key_gain,
    mixer_out,
    expert_input,
    norm_gain,
    routes,
    route_weights,
    w_gate,
    w_up,
    w_down,
):
    attended = attend(queries, keys, values, forget_cache, query_gain, key_gain)
    received, slots = dispatch(expert_input, norm_gain, routes)
    regrouped = lax.all_to_all(attended, "tp", split_axis=1, concat_axis=0, tiled=True)
    all_heads = regrouped.shape[0]
    projection = mixer_out.reshape(all_heads, regrouped.shape[2], mixer_out.shape[1])
    mixed = jnp.einsum(
        "hqd,hde->qe", regrouped, projection, preferred_element_type=jnp.float32
    ).astype(jnp.bfloat16)
    pieces = lax.all_gather(received, "tp", axis=0, tiled=True)
    gate = jnp.einsum("red,edf->ref", pieces, w_gate, preferred_element_type=jnp.float32)
    upward = jnp.einsum("red,edf->ref", pieces, w_up, preferred_element_type=jnp.float32)
    hidden = (jax.nn.silu(gate) * upward).astype(jnp.bfloat16)
    summed = lax.psum_scatter(
        jnp.einsum("ref,edf->red", hidden, w_down, preferred_element_type=jnp.float32).astype(
            jnp.bfloat16
        ),
        "tp",
        scatter_dimension=0,
        tiled=True,
    )
    returned = lax.all_to_all(summed, "ep", split_axis=0, concat_axis=1, tiled=True)
    flat_back = returned.reshape(-1, returned.shape[2])
    picked = (
        flat_back[slots]
        .reshape(routes.shape[0], routes.shape[1], returned.shape[2])
        .astype(jnp.float32)
    )
    routed = jnp.sum(picked * route_weights[:, :, None], axis=1).astype(jnp.bfloat16)
    return (mixed, routed)


def solution(mesh):
    in_specs = (
        P("ep", "tp"),
        P("ep", "tp"),
        P("ep", "tp"),
        P("tp", None),
        P(),
        P(),
        P(),
        P(("ep", "tp"), None),
        P(),
        P(("ep", "tp"), None),
        P(("ep", "tp"), None),
        P("ep", None, "tp"),
        P("ep", None, "tp"),
        P("ep", None, "tp"),
    )
    out_specs = (P(("ep", "tp"), None), P(("ep", "tp"), None))
    return jax.shard_map(
        on_device, mesh=mesh, in_specs=in_specs, out_specs=out_specs, check_vma=False
    )
```

profile of v0, /device:TPU:0, one launch (start us, length us, event | category | flops | bytes accessed | tf_op | source)
XLA Modules:
  0.0 367.3 jit_solution(14982361686460898123)
XLA Ops:
  7.2 0.8 copy.60
  9.4 1.4 scatter_custom_fusion
  10.8 1.2 fusion.22
  12.1 1.2 fusion.24
  13.4 2.5 gather_fusion.1
  15.8 1.2 copy.64
  17.0 55.3 %all_to_all.51 = bf16[16,32,2048]{2,0,1:T(8,128)(2,1)S(1)} all-to-all(bf16[16,32,2048]{2,0,1:T(8,128)(2,1)S(1)} %copy.64), channel_id=1, replica_groups=mesh['ep'=8,'tp'=4] {'ep'}, dimensions={1} | all-to-all | bytes 4194304 | tf_op jit(solution)/shard_map/all_to_all | solution.py:103
  72.3 1.5 copy.65
  73.9 0.8 copy-done
  74.9 0.8 fusion.30
  76.7 54.6 %all-gather.8.cloned.1.call-done = bf16[512,4,2048]{2,0,1:T(8,128)(2,1)} async-done(((bf16[128,4,2048]{2,0,1:T(8,128)(2,1)}), bf16[512,4,2048]{2,0,1:T(8,128)(2,1)}) %all-gather.8.cloned.1.call-update) | async-done | bytes 8388624 | tf_op jit(solution)/shard_map/all_gather | solution.py:131
  131.3 6.9 %fusion.42 = f32[4,512,256]{2,1,0:T(8,128)S(1)} fusion(bf16[512,4,2048]{2,0,1:T(8,128)(2,1)} %all-gather.8.cloned.1.call-done, bf16[4,2048,256]{2,1,0:T(8,128)(2,1)} %param.29), kind=kOutput, calls=%fused_computation.89 | convolution fusion | flops 2147483648 | bytes 14680064 | tf_op jit(solution)/shard_map/red,edf->ref/dot_general | solution.py:132
  138.2 14.0 %convert_bitcast_fusion = bf16[512,4,2048]{2,0,1:T(8,128)(2,1)} fusion(bf16[4,2048,256]{2,1,0:T(8,128)(2,1)} %param.31, f32[4,512,256]{2,1,0:T(8,128)S(1)} %fusion.42, bf16[512,4,2048]{2,0,1:T(8,128)(2,1)} %all-gather.8.cloned.1.call-done, bf16[4,2048,256]{2,1,0:T(8,128)(2,1)} %param.30), kind=kOutput, calls=%fused_computation.28 | convolution fusion | flops 4302307328 | bytes 27262976 | tf_op jit(solution)/shard_map/ref,edf->red/dot_general | solution.py:136
  154.2 1.0 gather_fusion
  156.1 18.2 %all-gather.4.cloned.1.call-done = bf16[4096,128]{1,0:T(8,128)(2,1)} async-done(((bf16[512,128]{1,0:T(8,128)(2,1)}), bf16[4096,128]{1,0:T(8,128)(2,1)}) %all-gather.4.cloned.1.call-update) | async-done | bytes 1048592 | tf_op jit(solution)/shard_map/all_gather | solution.py:40
  174.3 41.2 %all-gather.6.cloned.1.call-done = bf16[4096,128]{1,0:T(8,128)(2,1)} async-done(((bf16[512,128]{1,0:T(8,128)(2,1)}), bf16[4096,128]{1,0:T(8,128)(2,1)}) %all-gather.6.cloned.1.call-update) | async-done | bytes 1048592 | tf_op jit(solution)/shard_map/all_gather | solution.py:41
  215.5 8.8 %while.18 = (s32[]{:T(128)}, f32[2,512]{1,0:T(2,128)S(1)}, f32[2,512]{1,0:T(2,128)S(1)}, f32[2,512,128]{2,1,0:T(8,128)S(1)}, s32[]{:T(128)}, /*index=5*/bf16[409...) while((s32[]{:T(128)}, f32[2,512]{1,0:T(2,128)S(1)}, ...), condition=%wide.region_8.9_spmd.clone, body=%wide.region_3.8_spmd.clone.sunk | while | flops 274729984 | bytes 9007507 | solution.py:81
  216.1 4.0 %conditional.3 = ((f32[2,512]{1,0:T(2,128)S(1)}, f32[2,512]{1,0:T(2,128)S(1)}, f32[2,512,128]{2,1,0:T(8,128)S(1)})) conditional(s32[]{:T(128)} %convert_element_type.114, (f32[2,512]{1,0:T(2,128)S(1)}, f32[2,512]{1,0:T(2,128)S(1)}, f32[2,512,128]{2,1,0:T(8,128)S(1)}) %tuple.53, (s32[]{:T(128)}, s32[]{:T(128)}, s32[]{:T(128)}, ...), branch_computations={%region_4.4_spmd, %region_5.0_spmd} | conditional | flops 274729984 | bytes 9005188 | solution.py:79
  216.4 1.6 fusion.41
  218.4 1.7 convolution_add_fusion
  224.5 1.0 copy.58
  225.5 3.6 all-to-all-start
  229.1 58.9 %reduce-scatter.2.cloned.1.call-done = bf16[128,4,2048]{2,0,1:T(8,128)(2,1)} async-done(((bf16[512,4,2048]{2,0,1:T(8,128)(2,1)}), bf16[128,4,2048]{2,0,1:T(8,128)(2,1)}) %reduce-scatter.2.cloned.1.call-update) | async-done | bytes 2097168 | tf_op jit(solution)/shard_map/reduce_scatter | solution.py:135
  288.0 4.6 %copy.66 = bf16[128,4,2048]{2,1,0:T(4,128)(2,1)} copy(bf16[128,4,2048]{2,0,1:T(8,128)(2,1)} %reduce-scatter.2.cloned.1.call-done) | data formatting | bytes 4194304 | tf_op jit(solution)/shard_map/reduce_scatter | solution.py:135
  292.6 8.5 %all-to-all-start.2 = ((bf16[128,4,2048]{2,1,0:T(4,128)(2,1)}), bf16[128,4,2048]{2,1,0:T(4,128)(2,1)S(1)}, u32[]{:S(2)}, u32[]{:S(2)}) async-start(bf16[128,4,2048]{2,1,0:T(4,128)(2,1)} %copy.66), calls=%async_computation.3 | async-start | bytes 4194304 | tf_op jit(solution)/shard_map/all_to_all | solution.py:143
  301.2 3.7 %fusion.17 = bf16[128,2048]{1,0:T(8,128)(2,1)} fusion(bf16[8,128,128]{2,1,0:T(8,128)(2,1)S(1)} %bitcast.110, bf16[8,128,2048]{2,1,0:T(8,128)(2,1)} %bitcast.109), kind=kOutput, calls=%fused_computation.30 | convolution fusion | flops 537133056 | bytes 4980736 | tf_op jit(solution)/shard_map/hqd,hde->qe/dot_general | solution.py:128
  304.9 44.2 %all-to-all-done.2 = bf16[128,4,2048]{2,1,0:T(4,128)(2,1)S(1)} async-done(((bf16[128,4,2048]{2,1,0:T(4,128)(2,1)}), bf16[128,4,2048]{2,1,0:T(4,128)(2,1)S(1)}, u32[]{:S(2)}, u32[]{:S(2)}) %all-to-all-start.2) | async-done | bytes 2097184 | tf_op jit(solution)/shard_map/all_to_all | solution.py:143
  349.1 2.4 copy.73
  351.5 2.5 reshape.156
  354.0 1.4 gather_fusion.2
  355.4 1.3 reshape.158
  356.7 4.0 %multiply_reduce_fusion = bf16[128,2048]{1,0:T(8,128)(2,1)} fusion(f32[128,2,2048]{2,1,0:T(2,128)S(1)} %reshape.158, f32[128,2]{1,0:T(8,128)S(1)} %copy.68), kind=kLoop, calls=%fused_computation.39 | loop fusion | flops 786432 | bytes 2622464 | tf_op jit(solution)/shard_map/reduce_sum | solution.py:150
  (79 shorter events, 6.6 us)
Async XLA Ops:
  7.2 124.1 %all-gather.8.cloned.1.call-start = ((), (), s32[]{:S(2)}) async-start(), calls=%async_computation.6 | async-start | bytes 10485760 | tf_op jit(solution)/shard_map/all_gather | solution.py:131
  73.8 0.9 copy-start
  73.8 1.1 copy-start.4
  73.8 100.4 %all-gather.4.cloned.1.call-start = ((), (), s32[]{:S(2)}) async-start(), calls=%async_computation.4 | async-start | bytes 1179648 | tf_op jit(solution)/shard_map/all_gather | solution.py:40
  75.7 139.7 %all-gather.6.cloned.1.call-start = ((), (), s32[]{:S(2)}) async-start(), calls=%async_computation.5 | async-start | bytes 1179648 | tf_op jit(solution)/shard_map/all_gather | solution.py:41
  76.5 211.6 %reduce-scatter.2.cloned.1.call-start = ((), (), s32[]{:S(2)}) async-start(), calls=%async_computation.7 | async-start | bytes 10485760 | tf_op jit(solution)/shard_map/reduce_scatter | solution.py:135
  152.2 0.8 copy-start.2
  152.2 3.3 copy-start.1
  152.2 3.6 copy-start.5
  225.5 67.1 %all-to-all-start = ((bf16[2,512,128]{2,0,1:T(2,128)(2,1)}), bf16[2,512,128]{2,0,1:T(2,128)(2,1)S(1)}, u32[]{:S(2)}, u32[]{:S(2)}) async-start(bf16[2,512,128]{2,0,1:T(2,128)(2,1)} %copy.58), calls=%async_computation | async-start | bytes 524288 | tf_op jit(solution)/shard_map/all_to_all | solution.py:125
  292.6 8.5 %copy-start.3 = (f32[128,2]{0,1:T(2,128)S(1)}, f32[128,2]{0,1:T(2,128)}, u32[]{:S(2)}) copy-start(f32[128,2]{0,1:T(2,128)} %param.28) | copy-start | bytes 3076
  292.6 56.5 %all-to-all-start.2 = ((bf16[128,4,2048]{2,1,0:T(4,128)(2,1)}), bf16[128,4,2048]{2,1,0:T(4,128)(2,1)S(1)}, u32[]{:S(2)}, u32[]{:S(2)}) async-start(bf16[128,4,2048]{2,1,0:T(4,128)(2,1)} %copy.66), calls=%async_computation.3 | async-start | bytes 4194304 | tf_op jit(solution)/shard_map/all_to_all | solution.py:143
Sparse Core Ops, SparseCore 0:
  74.0 57.2 all-gather.7
  134.0 40.2 all-gather.3
  176.4 38.9 all-gather.5
  217.9 70.0 reduce-scatter.1
where the time goes:
time: 368 us; the launch traced here: 367 us
  waiting for transfers between devices  218 us (59%)
  blocking collectives  55.3 us (15%)
  matrix products  27.9 us (8%)
  local copies, waits for them, and re-layouts  25 us (7%)
  between operations  14 us (4%)
  starting transfers between devices  12.5 us (3%)
  other arithmetic  10.1 us (3%)
  loops' own time  4.82 us (1%)
    reduce_scatter x1, waiting for transfers between devices, on_device(): lax.psum_scatter(jnp.einsum('ref,edf->red', hidden, w_down, preferred_ele...  58.9 us
    all_to_all x1, blocking collectives, dispatch(): lax.all_to_all(outgoing, 'ep', split_axis=1, concat_axis=0, tiled=True)  55.3 us
    all_gather x1, waiting for transfers between devices, on_device(): pieces = lax.all_gather(received, 'tp', axis=0, tiled=True)  54.6 us
    all_to_all x1, waiting for transfers between devices, on_device(): lax.all_to_all(summed, 'ep', split_axis=0, concat_axis=1, tiled=True)  44.2 us
    all_gather x1, waiting for transfers between devices, attend(): value_rows = lax.all_gather(values, 'ep', axis=0, tiled=True)  41.2 us
    all_gather x1, waiting for transfers between devices, attend(): key_matrix_rows = lax.all_gather(normed_k, 'ep', axis=0, tiled=True)  18.2 us
    dot_general x1, matrix products, on_device(): jnp.einsum('ref,edf->red', hidden, w_down, preferred_element_type=jnp.flo...  14 us
    all_to_all x1, starting transfers between devices, on_device(): lax.all_to_all(summed, 'ep', split_axis=0, concat_axis=1, tiled=True)  8.48 us
  transfers between devices with their start and end apart: 6, of which 5 were waited for; matrix products, arithmetic and copies ran while one was open for 10% of the time, Pallas kernels for 0%

commit v1 on v0

--- a/solution.py
+++ b/solution.py
@@ -128,7 +128,12 @@
     mixed = jnp.einsum(
         "hqd,hde->qe", regrouped, projection, preferred_element_type=jnp.float32
     ).astype(jnp.bfloat16)
-    pieces = lax.all_gather(received, "tp", axis=0, tiled=True)
+    ring = [received]
+    for hop in range(3):
+        ring.append(lax.ppermute(ring[-1], "tp", [(dev, (dev + 1) % 4) for dev in range(4)]))
+    pieces = jnp.roll(
+        jnp.concatenate(ring[::-1], axis=0), (lax.axis_index("tp") + 1) * ring[0].shape[0], axis=0
+    )
     gate = jnp.einsum("red,edf->ref", pieces, w_gate, preferred_element_type=jnp.float32)
     upward = jnp.einsum("red,edf->ref", pieces, w_up, preferred_element_type=jnp.float32)
     hidden = (jax.nn.silu(gate) * upward).astype(jnp.bfloat16)

time: 368 us -> 335 us (0.910)
  waiting for transfers between devices: 218 us -> 175 us
  local copies, waits for them, and re-layouts: 25 us -> 38.4 us
  starting transfers between devices: 12.5 us -> 8.74 us
    ppermute x0 -> x3, waiting for transfers between devices: none -> 74.8 us  [on_device(): lax.ppermute(ring[-1], 'tp', [(dev, (dev + 1) % 4) for dev in range(4)])]
    all_gather x1 -> x0, waiting for transfers between devices: 54.6 us -> none  [on_device(): pieces = lax.all_gather(received, 'tp', axis=0, tiled=True)]
    reduce_scatter x1, waiting for transfers between devices: 58.9 us -> 35.3 us  [on_device(): lax.psum_scatter(jnp.einsum('ref,edf->red', hidden, w_down, preferred_ele...]
    all_gather x1, waiting for transfers between devices: 41.2 us -> 19.6 us  [attend(): value_rows = lax.all_gather(values, 'ep', axis=0, tiled=True)]
    all_gather x1, waiting for transfers between devices: 18.2 us -> 0.02 us  [attend(): key_matrix_rows = lax.all_gather(normed_k, 'ep', axis=0, tiled=True)]
    unnamed x18 -> x31, local copies, waits for them, and re-layouts: 3.55 us -> 17.8 us
    all_to_all x1, starting transfers between devices: 8.48 us -> 4.74 us  [on_device(): lax.all_to_all(summed, 'ep', split_axis=0, concat_axis=1, tiled=True)]
  transfers between devices with their start and end apart: 6 -> 8, of which waited for: 5 -> 6; matrix products, arithmetic and copies ran while one was open for 10% -> 13% of each run, Pallas kernels for 0% -> 0%
where the time goes in v1:
time: 335 us; the launch traced here: 334 us
  waiting for transfers between devices  175 us (52%)
  blocking collectives  55.3 us (17%)
  local copies, waits for them, and re-layouts  38.4 us (11%)
  matrix products  25.4 us (8%)
  between operations  15.9 us (5%)
  other arithmetic  10 us (3%)
  starting transfers between devices  8.74 us (3%)
  loops' own time  5.28 us (2%)
    ppermute x3, waiting for transfers between devices, on_device(): lax.ppermute(ring[-1], 'tp', [(dev, (dev + 1) % 4) for dev in range(4)])  74.8 us
    all_to_all x1, blocking collectives, dispatch(): lax.all_to_all(outgoing, 'ep', split_axis=1, concat_axis=0, tiled=True)  55.3 us
    all_to_all x1, waiting for transfers between devices, on_device(): lax.all_to_all(summed, 'ep', split_axis=0, concat_axis=1, tiled=True)  44.1 us
    reduce_scatter x1, waiting for transfers between devices, on_device(): lax.psum_scatter(jnp.einsum('ref,edf->red', hidden, w_down, preferred_ele...  35.3 us
    all_gather x1, waiting for transfers between devices, attend(): value_rows = lax.all_gather(values, 'ep', axis=0, tiled=True)  19.6 us
    unnamed x31, local copies, waits for them, and re-layouts  17.8 us
    dot_general x1, matrix products, on_device(): jnp.einsum('ref,edf->red', hidden, w_down, preferred_element_type=jnp.flo...  13.8 us
  transfers between devices with their start and end apart: 8, of which 6 were waited for; matrix products, arithmetic and copies ran while one was open for 13% of the time, Pallas kernels for 0%

profile of v1, /device:TPU:0, one launch (start us, length us, event | category | flops | bytes accessed | tf_op | source)
XLA Modules:
  0.0 333.6 jit_solution(10587660526966371674)
XLA Ops:
  10.2 1.4 scatter_custom_fusion
  11.7 1.2 fusion.28
  12.9 1.2 fusion.30
  14.2 2.5 gather_fusion.1
  17.8 55.3 %all_to_all.51 = bf16[16,32,2048]{2,0,1:T(8,128)(2,1)S(1)} all-to-all(bf16[16,32,2048]{2,0,1:T(8,128)(2,1)S(1)} %copy.64), channel_id=1, replica_groups=mesh['ep'=8,'tp'=4] {'ep'}, dimensions={1} | all-to-all | bytes 4194304 | tf_op jit(solution)/shard_map/all_to_all | solution.py:103
  73.4 25.4 %collective-permute-done = bf16[128,4,2048]{2,0,1:T(8,128)(2,1)S(1)} collective-permute-done((bf16[128,4,2048]{2,0,1:T(8,128)(2,1)S(1)}, bf16[128,4,2048]{2,0,1:T(8,128)(2,1)S(1)}, u32[]{:S(2)}, u32[]{:S(2)}) %collective-permute-start) | collective-permute-done | bytes 2097184 | tf_op jit(solution)/shard_map/ppermute | solution.py:133
  98.8 1.3 copy-done
  100.3 25.4 %collective-permute-done.1 = bf16[128,4,2048]{2,0,1:T(8,128)(2,1)} collective-permute-done((bf16[128,4,2048]{2,0,1:T(8,128)(2,1)S(1)}, bf16[128,4,2048]{2,0,1:T(8,128)(2,1)}, u32[]{:S(2)}, u32[]{:S(2)}) %collective-permute-start.1) | collective-permute-done | bytes 2097184 | tf_op jit(solution)/shard_map/ppermute | solution.py:133
  127.5 23.9 %collective-permute-done.2 = bf16[128,4,2048]{2,0,1:T(8,128)(2,1)} collective-permute-done((bf16[128,4,2048]{2,0,1:T(8,128)(2,1)}, bf16[128,4,2048]{2,0,1:T(8,128)(2,1)}, u32[]{:S(2)}, u32[]{:S(2)}) %collective-permute-start.2) | collective-permute-done | bytes 2097184 | tf_op jit(solution)/shard_map/ppermute | solution.py:133
  151.5 1.8 constant_dynamic-update-slice_fusion.7
  153.3 2.0 constant_dynamic-update-slice_fusion.6
  155.8 1.8 constant_dynamic-update-slice_fusion.3
  157.6 1.8 constant_dynamic-update-slice_fusion.2
  159.8 5.7 %copy-done.3 = bf16[1024,4,2048]{2,0,1:T(8,128)(2,1)} copy-done((bf16[1024,4,2048]{2,0,1:T(8,128)(2,1)}, bf16[1024,4,2048]{2,0,1:T(8,128)(2,1)S(1)}, u32[]{:S(2)}) %copy-start.3) | copy-done | bytes 16777240
  165.5 4.5 %fusion.19 = f32[4,512,256]{2,1,0:T(8,128)S(1)} fusion(bf16[4,2048,256]{2,1,0:T(8,128)(2,1)} %param.29, bf16[1024,4,2048]{2,0,1:T(8,128)(2,1)S(1)} %constant_dynamic-update-slice_fusion, s32[]{:T(128)S(6)} %select_n.73), kind=kOutput, calls=%fused_computation.31 | convolution fusion | flops 2147483648 | bytes 14680068 | tf_op jit(solution)/shard_map/red,edf->ref/dot_general | solution.py:137
  170.1 13.8 %convert_bitcast_fusion = bf16[512,4,2048]{2,0,1:T(8,128)(2,1)} fusion(bf16[4,2048,256]{2,1,0:T(8,128)(2,1)} %param.31, f32[4,512,256]{2,1,0:T(8,128)S(1)} %fusion.19, bf16[4,2048,256]{2,1,0:T(8,128)(2,1)} %param.30, bf16[1024,4,2048]{2,0,1:T(8,128)(2,1)} %copy-done.3, s32[]{:T(128)S(6)} %select_n.73), kind=kOutput, calls=%fused_computation.28 | convolution fusion | flops 4302307328 | bytes 27262980 | tf_op jit(solution)/shard_map/ref,edf->red/dot_general | solution.py:141
  187.8 19.6 %all-gather.5.cloned.1.call-done = bf16[4096,128]{1,0:T(8,128)(2,1)} async-done(((bf16[512,128]{1,0:T(8,128)(2,1)}), bf16[4096,128]{1,0:T(8,128)(2,1)}) %all-gather.5.cloned.1.call-update) | async-done | bytes 1048592 | tf_op jit(solution)/shard_map/all_gather | solution.py:41
  207.5 9.3 %while.18 = (s32[]{:T(128)}, f32[2,512]{1,0:T(2,128)S(1)}, f32[2,512]{1,0:T(2,128)S(1)}, f32[2,512,128]{2,1,0:T(8,128)S(1)}, s32[]{:T(128)}, /*index=5*/bf16[409...) while((s32[]{:T(128)}, f32[2,512]{1,0:T(2,128)S(1)}, ...), condition=%wide.region_8.9_spmd.clone, body=%wide.region_3.8_spmd.clone.sunk | while | flops 274729984 | bytes 9007507 | solution.py:81
  208.1 4.1 %conditional.3 = ((f32[2,512]{1,0:T(2,128)S(1)}, f32[2,512]{1,0:T(2,128)S(1)}, f32[2,512,128]{2,1,0:T(8,128)S(1)})) conditional(s32[]{:T(128)} %convert_element_type.112, (f32[2,512]{1,0:T(2,128)S(1)}, f32[2,512]{1,0:T(2,128)S(1)}, f32[2,512,128]{2,1,0:T(8,128)S(1)}) %tuple.54, (s32[]{:T(128)}, s32[]{:T(128)}, s32[]{:T(128)}, ...), branch_computations={%region_4.4_spmd, %region_5.0_spmd} | conditional | flops 274729984 | bytes 9005188 | solution.py:79
  208.4 1.6 fusion.53
  210.5 1.7 convolution_add_fusion
  218.0 3.6 %all-to-all-start = ((bf16[2,512,128]{2,0,1:T(2,128)(2,1)}), bf16[2,512,128]{2,0,1:T(2,128)(2,1)S(1)}, u32[]{:S(2)}, u32[]{:S(2)}) async-start(bf16[2,512,128]{2,0,1:T(2,128)(2,1)} %copy.58), calls=%async_computation | async-start | bytes 524288 | tf_op jit(solution)/shard_map/all_to_all | solution.py:125
  221.6 35.3 %reduce-scatter.2.cloned.1.call-done = bf16[128,4,2048]{2,0,1:T(8,128)(2,1)} async-done(((bf16[512,4,2048]{2,0,1:T(8,128)(2,1)}), bf16[128,4,2048]{2,0,1:T(8,128)(2,1)}) %reduce-scatter.2.cloned.1.call-update) | async-done | bytes 2097168 | tf_op jit(solution)/shard_map/reduce_scatter | solution.py:140
  256.9 4.5 %copy.66 = bf16[128,4,2048]{2,1,0:T(4,128)(2,1)} copy(bf16[128,4,2048]{2,0,1:T(8,128)(2,1)} %reduce-scatter.2.cloned.1.call-done) | data formatting | bytes 4194304 | tf_op jit(solution)/shard_map/reduce_scatter | solution.py:140
  261.4 4.7 %all-to-all-start.2 = ((bf16[128,4,2048]{2,1,0:T(4,128)(2,1)}), bf16[128,4,2048]{2,1,0:T(4,128)(2,1)S(1)}, u32[]{:S(2)}, u32[]{:S(2)}) async-start(bf16[128,4,2048]{2,1,0:T(4,128)(2,1)} %copy.66), calls=%async_computation.3 | async-start | bytes 4194304 | tf_op jit(solution)/shard_map/all_to_all | solution.py:148
  266.3 3.7 %fusion.21 = bf16[128,2048]{1,0:T(8,128)(2,1)} fusion(bf16[8,128,128]{2,1,0:T(8,128)(2,1)S(1)} %bitcast.97, bf16[8,128,2048]{2,1,0:T(8,128)(2,1)} %bitcast.96), kind=kOutput, calls=%fused_computation.34 | convolution fusion | flops 537133056 | bytes 4980736 | tf_op jit(solution)/shard_map/hqd,hde->qe/dot_general | solution.py:128
  270.1 44.1 %all-to-all-done.2 = bf16[128,4,2048]{2,1,0:T(4,128)(2,1)S(1)} async-done(((bf16[128,4,2048]{2,1,0:T(4,128)(2,1)}), bf16[128,4,2048]{2,1,0:T(4,128)(2,1)S(1)}, u32[]{:S(2)}, u32[]{:S(2)}) %all-to-all-start.2) | async-done | bytes 2097184 | tf_op jit(solution)/shard_map/all_to_all | solution.py:148
  314.2 2.7 copy.73
  316.9 2.5 reshape.156
  319.5 1.4 gather_fusion.2
  320.9 1.3 reshape.158
  322.2 3.9 %multiply_reduce_fusion = bf16[128,2048]{1,0:T(8,128)(2,1)} fusion(f32[128,2,2048]{2,1,0:T(2,128)S(1)} %reshape.158, f32[128,2]{1,0:T(8,128)S(1)} %copy.68), kind=kLoop, calls=%fused_computation.43 | loop fusion | flops 786432 | bytes 2622464 | tf_op jit(solution)/shard_map/reduce_sum | solution.py:155
  (95 shorter events, 12.4 us)
Async XLA Ops:
  8.0 179.8 %all-gather.3.cloned.1.call-start = ((), (), s32[]{:S(2)}) async-start(), calls=%async_computation.4 | async-start | bytes 1179648 | tf_op jit(solution)/shard_map/all_gather | solution.py:40
  73.2 27.0 %copy-start.2 = (bf16[512,128]{1,0:T(8,128)(2,1)S(1)}, bf16[512,128]{1,0:T(8,128)(2,1)}, u32[]{:S(2)}) copy-start(bf16[512,128]{1,0:T(8,128)(2,1)} %param.19) | copy-start | bytes 393220
  73.2 52.5 %copy-start.7 = (f32[128]{0:T(128)S(1)}, f32[128]{0:T(128)}, u32[]{:S(2)}) copy-start(f32[128]{0:T(128)} %param.23) | copy-start | bytes 1540
  73.3 25.5 %collective-permute-start = (bf16[128,4,2048]{2,0,1:T(8,128)(2,1)S(1)}, bf16[128,4,2048]{2,0,1:T(8,128)(2,1)S(1)}, u32[]{:S(2)}, u32[]{:S(2)}) collective-permute-start(bf16[128,4,2048]{2,0,1:T(8,128)(2,1)S(1)} %bitcast.89), channel_id=1, source_target_pairs={{0,1},{1,2},{2,3},{3,0},{4,5},{5,6},{6,7},{7,4},{8,9},{9,10},{10,1... | collective-permute-start | bytes 6291464 | tf_op jit(solution)/shard_map/ppermute | solution.py:133
  98.8 1.3 copy-start
  100.1 25.6 %collective-permute-start.1 = (bf16[128,4,2048]{2,0,1:T(8,128)(2,1)S(1)}, bf16[128,4,2048]{2,0,1:T(8,128)(2,1)}, u32[]{:S(2)}, u32[]{:S(2)}) collective-permute-start(bf16[128,4,2048]{2,0,1:T(8,128)(2,1)S(1)} %collective-permute-done), channel_id=1, source_target_pairs={{0,1},{1,2},{2,3},{3,0},{4,5},{5,6},{6,7},{7,4},{8,9},{9,10},{10,1... | collective-permute-start | bytes 6291464 | tf_op jit(solution)/shard_map/ppermute | solution.py:133
  125.7 25.8 %collective-permute-start.2 = (bf16[128,4,2048]{2,0,1:T(8,128)(2,1)}, bf16[128,4,2048]{2,0,1:T(8,128)(2,1)}, u32[]{:S(2)}, u32[]{:S(2)}) collective-permute-start(bf16[128,4,2048]{2,0,1:T(8,128)(2,1)} %collective-permute-done.1), channel_id=1, source_target_pairs={{0,1},{1,2},{2,3},{3,0},{4,5},{5,6},{6,7},{7,4},{8,9},{9,10},{10,1... | collective-permute-start | bytes 6291464 | tf_op jit(solution)/shard_map/ppermute | solution.py:133
  126.5 80.9 %all-gather.5.cloned.1.call-start = ((), (), s32[]{:S(2)}) async-start(), calls=%async_computation.5 | async-start | bytes 1179648 | tf_op jit(solution)/shard_map/all_gather | solution.py:41
  127.3 129.7 %reduce-scatter.2.cloned.1.call-start = ((), (), s32[]{:S(2)}) async-start(), calls=%async_computation.6 | async-start | bytes 10485760 | tf_op jit(solution)/shard_map/reduce_scatter | solution.py:140
  153.3 2.2 copy-start.1
  159.8 5.7 %copy-start.3 = (bf16[1024,4,2048]{2,0,1:T(8,128)(2,1)}, bf16[1024,4,2048]{2,0,1:T(8,128)(2,1)S(1)}, u32[]{:S(2)}) copy-start(bf16[1024,4,2048]{2,0,1:T(8,128)(2,1)S(1)} %constant_dynamic-update-slice_fusion) | copy-start | bytes 50331652
  183.8 0.8 copy-start.5
  183.9 3.4 %copy-start.4 = (bf16[512,256]{1,0:T(8,128)(2,1)S(1)}, bf16[512,256]{1,0:T(8,128)(2,1)}, u32[]{:S(2)}) copy-start(bf16[512,256]{1,0:T(8,128)(2,1)} %param.18) | copy-start | bytes 786436
  183.9 3.6 %copy-start.8 = (f32[128]{0:T(128)S(1)}, f32[128]{0:T(128)}, u32[]{:S(2)}) copy-start(f32[128]{0:T(128)} %param.22) | copy-start | bytes 1540
  218.0 43.4 %all-to-all-start = ((bf16[2,512,128]{2,0,1:T(2,128)(2,1)}), bf16[2,512,128]{2,0,1:T(2,128)(2,1)S(1)}, u32[]{:S(2)}, u32[]{:S(2)}) async-start(bf16[2,512,128]{2,0,1:T(2,128)(2,1)} %copy.58), calls=%async_computation | async-start | bytes 524288 | tf_op jit(solution)/shard_map/all_to_all | solution.py:125
  261.4 4.8 %copy-start.6 = (f32[128,2]{0,1:T(2,128)S(1)}, f32[128,2]{0,1:T(2,128)}, u32[]{:S(2)}) copy-start(f32[128,2]{0,1:T(2,128)} %param.28) | copy-start | bytes 3076
  261.4 52.8 %all-to-all-start.2 = ((bf16[128,4,2048]{2,1,0:T(4,128)(2,1)}), bf16[128,4,2048]{2,1,0:T(4,128)(2,1)S(1)}, u32[]{:S(2)}, u32[]{:S(2)}) async-start(bf16[128,4,2048]{2,1,0:T(4,128)(2,1)} %copy.66), calls=%async_computation.3 | async-start | bytes 4194304 | tf_op jit(solution)/shard_map/all_to_all | solution.py:148
Sparse Core Ops, SparseCore 0:
  126.6 39.6 all-gather.2
  168.4 38.9 all-gather.4
Sparse Core Ops, SparseCore 1:
  183.9 72.9 reduce-scatter.1
